TPU v7x, 32 devices: a whole 2x2x4 slice. The times are simulated.
32 devices in a mesh: ra: 8 (over z, y), cb: 4 (over x, core).
Axes of the slice: x: 2, y: 2, z: 4, core: 2. Of those that a mesh axis runs over, the one named last changes fastest.
Arguments:
- tokens: bfloat16 [512, 4096], P(None, 'cb'), may hold values from -400 to 400
- norm_gain: bfloat16 [4096], P('cb'), may hold values from 0.099609375 to 1.8984375
- w_gate: bfloat16 [4096, 11264], P('cb', 'ra'), may hold values from -0.09375 to 0.09375
- w_up: bfloat16 [4096, 11264], P('cb', 'ra'), may hold values from -0.09375 to 0.09375
- w_down: bfloat16 [11264, 4096], P('ra', 'cb'), may hold values from -0.0546875 to 0.0546875
- out_gain: bfloat16 [4096], P('cb'), may hold values from 0.099609375 to 1.8984375
Outputs:
- normed_out: bfloat16 [512, 4096], P('ra', 'cb')
All inputs are finite; a program needn't handle non-finite values.
Results may differ from a plain program's by a relative error of at most 0.0045.
Values sent between devices are 32-bit elements; how exact they have to be, the bound alone decides.
A program may use at most 64 MiB of HBM per device.

v0:
```python
import jax
import jax.numpy as jnp
from jax import lax
from jax.sharding import PartitionSpec as P

D = 4096


def body(tokens, norm_gain, w_gate, w_up, w_down, out_gain):
    eps = 1e-06
    xfloat = tokens.astype(jnp.float32)
    local_sq = jnp.sum(xfloat * xfloat, axis=1)
    scaled = (xfloat * norm_gain.astype(jnp.float32)).astype(jnp.bfloat16)
    gate_part = jnp.dot(scaled, w_gate, preferred_element_type=jnp.float32)
    up_part = jnp.dot(scaled, w_up, preferred_element_type=jnp.float32)
    total_sq, gate_sum, up_sum = lax.psum((local_sq, gate_part, up_part), "cb")
    inv_in = lax.rsqrt(total_sq / D + eps)[:, None]
    hidden = (jax.nn.silu(gate_sum * inv_in) * (up_sum * inv_in)).astype(jnp.bfloat16)
    partial_down = jnp.dot(hidden, w_down, preferred_element_type=jnp.float32)
    own_rows = tokens.shape[0] // lax.axis_size("ra")
    first_row = lax.axis_index("ra") * own_rows
    down = lax.psum_scatter(partial_down, "ra", scatter_dimension=0, tiled=True)
    residual = lax.dynamic_slice_in_dim(xfloat, first_row, own_rows, 0)
    mixed = 0.1 * residual + down
    out_sq = lax.psum(jnp.sum(mixed * mixed, axis=1), "cb")
    inv_out = lax.rsqrt(out_sq / D + eps)[:, None]
    return (mixed * inv_out * out_gain.astype(jnp.float32)).astype(jnp.bfloat16)


def solution(mesh):
    return jax.shard_map(
        body,
        mesh=mesh,
        in_specs=(P(None, "cb"), P("cb"), P("cb", "ra"), P("cb", "ra"), P("ra", "cb"), P("cb")),
        out_specs=P("ra", "cb"),
        check_vma=False,
    )
```

profile of v0, /device:TPU:0, one launch (start us, length us, event | category | flops | bytes accessed | tf_op | source)
XLA Modules:
  0.0 221.7 jit_solution(3549083786909565861)
XLA Ops:
  6.5 0.0 copy-start
  6.5 0.0 all-reduce.3.cloned.1.call-start
  6.5 0.8 convert_element_type.19
  7.4 1.0 copy-done
  8.4 0.0 copy-start.1
  8.4 0.0 copy-start.3
  8.4 4.7 %fusion.1 = f32[512,1408]{1,0:T(8,128)} fusion(bf16[1024,1408]{1,0:T(8,128)(2,1)S(1)} %copy-done, f32[1024]{0:T(1024)S(1)} %convert_element_type.19, bf16[512,1024]{1,0:T(8,128)(2,1)} %param.6), kind=kOutput, calls=%fused_computation.4 | convolution fusion | flops 1477967872 | bytes 6819840 | tf_op jit(solution)/shard_map/dot_general | solution.py:15
  13.1 0.0 copy-done.1
  13.1 0.0 copy-done.3
  13.1 3.5 %fusion.2 = f32[512,1408]{1,0:T(8,128)} fusion(bf16[1024,1408]{1,0:T(8,128)(2,1)S(1)} %copy-done.3, f32[1024]{0:T(1024)S(1)} %convert_element_type.19, bf16[512,1024]{1,0:T(8,128)(2,1)S(1)} %copy-done.1), kind=kOutput, calls=%fused_computation.5 | convolution fusion | flops 1477967872 | bytes 6819840 | tf_op jit(solution)/shard_map/dot_general | solution.py:14
  16.6 0.0 all-reduce.3.cloned.1.call-update
  16.6 0.0 reduce-scatter.2.cloned.1.call-start
  16.6 1.5 multiply_reduce_fusion
  18.1 8.4 %psum.29 = f32[512]{0:T(512)S(1)} all-reduce(f32[512]{0:T(512)S(1)} %multiply_reduce_fusion), channel_id=1, replica_groups=mesh['ra'=8,'cb'=4] {'cb'}, use_global_device_ids=true, to_apply=%region_2.0 | all-reduce | flops 512 | bytes 4096 | tf_op jit(solution)/shard_map/psum | solution.py:16
  26.5 104.0 %all-reduce.3.cloned.1.call-done = (f32[512,1408]{1,0:T(8,128)}, f32[512,1408]{1,0:T(8,128)}) async-done(((f32[512,1408]{1,0:T(8,128)}, f32[512,1408]{1,0:T(8,128)}), (f32[512,1408]{1,0:T(8,128)}, f32[512,1408]{1,0:T(8,128)})) %all-reduce.3.cloned.1.call-update) | async-done | bytes 5767184 | tf_op jit(solution)/shard_map/psum | solution.py:16
  130.5 6.8 %fusion = f32[512,1024]{1,0:T(8,128)} fusion(bf16[1408,1024]{1,0:T(8,128)(2,1)} %param.10, f32[512,1408]{1,0:T(8,128)} %get-tuple-element.5, f32[512,1408]{1,0:T(8,128)} %get-tuple-element.6, f32[512]{0:T(512)S(1)} %add_rsqrt_fusion), kind=kOutput, calls=%fused_computation.3 | convolution fusion | flops 1482162176 | bytes 10749952 | tf_op jit(solution)/shard_map/dot_general | solution.py:19
  137.4 0.0 copy-start.2
  137.4 0.0 reduce-scatter.2.cloned.1.call-update
  137.4 2.8 %convert_element_type.18 = f32[512,1024]{1,0:T(8,128)} convert(bf16[512,1024]{1,0:T(8,128)(2,1)} %param.6) | non-fusion elementwise | flops 524288 | bytes 3145728 | tf_op jit(solution)/shard_map/convert_element_type | solution.py:11
  140.2 0.0 copy-done.2
  140.2 66.0 %reduce-scatter.2.cloned.1.call-done = f32[64,1024]{1,0:T(8,128)} async-done(((f32[512,1024]{1,0:T(8,128)}), f32[64,1024]{1,0:T(8,128)}) %reduce-scatter.2.cloned.1.call-update) | async-done | bytes 262160 | tf_op jit(solution)/shard_map/reduce_scatter | solution.py:22
  206.2 1.2 multiply_reduce_fusion.1
  207.4 5.7 %psum.31 = f32[64]{0:T(128)S(1)} all-reduce(f32[64]{0:T(128)S(1)} %multiply_reduce_fusion.1), channel_id=1, replica_groups=mesh['ra'=8,'cb'=4] {'cb'}, use_global_device_ids=true, to_apply=%region_6.7 | all-reduce | flops 64 | bytes 512 | tf_op jit(solution)/shard_map/psum | solution.py:25
  213.0 1.8 multiply_convert_fusion.5
  (3 shorter events, 0.0 us)
Async XLA Ops:
  6.5 1.8 copy-start
  6.5 124.0 %all-reduce.3.cloned.1.call-start = ((), (), s32[]{:S(2)}) async-start(), calls=%async_computation.2 | async-start | bytes 11534336 | tf_op jit(solution)/shard_map/psum | solution.py:16
  8.4 4.7 %copy-start.1 = (bf16[512,1024]{1,0:T(8,128)(2,1)S(1)}, bf16[512,1024]{1,0:T(8,128)(2,1)}, u32[]{:S(2)}) copy-start(bf16[512,1024]{1,0:T(8,128)(2,1)} %param.6) | copy-start | bytes 3145732
  8.4 4.7 %copy-start.3 = (bf16[1024,1408]{1,0:T(8,128)(2,1)S(1)}, bf16[1024,1408]{1,0:T(8,128)(2,1)}, u32[]{:S(2)}) copy-start(bf16[1024,1408]{1,0:T(8,128)(2,1)} %param.8) | copy-start | bytes 8650756
  16.6 189.6 %reduce-scatter.2.cloned.1.call-start = ((), (), s32[]{:S(2)}) async-start(), calls=%async_computation.1 | async-start | bytes 2359296 | tf_op jit(solution)/shard_map/reduce_scatter | solution.py:22
  137.4 2.9 %copy-start.2 = (bf16[1024]{0:T(1024)(128)(2,1)S(1)}, bf16[1024]{0:T(1024)(128)(2,1)}, u32[]{:S(2)}) copy-start(bf16[1024]{0:T(1024)(128)(2,1)} %param.11) | copy-start | bytes 6148
Sparse Core Ops, SparseCore 0:
  16.7 113.7 all-reduce.2
  137.5 68.6 reduce-scatter.1
where the time goes:
time: 222 us
  waiting for transfers between devices  170 us (77%)
  matrix products  15 us (7%)
  blocking collectives  14 us (6%)
  between operations  13.4 us (6%)
  other arithmetic  8.13 us (4%)
    psum x1, waiting for transfers between devices, body(): total_sq, gate_sum, up_sum = lax.psum((local_sq, gate_part, up_part), 'cb')  104 us
    reduce_scatter x1, waiting for transfers between devices, body(): down = lax.psum_scatter(partial_down, 'ra', scatter_dimension=0, tiled=True)  66 us
    psum x1, blocking collectives, body(): total_sq, gate_sum, up_sum = lax.psum((local_sq, gate_part, up_part), 'cb')  8.37 us
    dot_general x1, matrix products, body(): partial_down = jnp.dot(hidden, w_down, preferred_element_type=jnp.float32)  6.83 us
    psum x1, blocking collectives, body(): out_sq = lax.psum(jnp.sum(mixed * mixed, axis=1), 'cb')  5.67 us
    dot_general x1, matrix products, body(): up_part = jnp.dot(scaled, w_up, preferred_element_type=jnp.float32)  4.74 us
  transfers between devices with their start and end apart: 2, of which 2 were waited for; matrix products, arithmetic and copies ran while one was open for 2% of the time, Pallas kernels for 0%

commit v1 on v0

--- a/solution.py
+++ b/solution.py
@@ -4,6 +4,11 @@
 from jax.sharding import PartitionSpec as P
 
 D = 4096
+
+
+def _direct_rails(array_here):
+    res = lax.all_gather(array_here, "cb").sum(axis=0)
+    return res
 
 
 def body(tokens, norm_gain, w_gate, w_up, w_down, out_gain):
@@ -22,7 +27,7 @@
     down = lax.psum_scatter(partial_down, "ra", scatter_dimension=0, tiled=True)
     residual = lax.dynamic_slice_in_dim(xfloat, first_row, own_rows, 0)
     mixed = 0.1 * residual + down
-    out_sq = lax.psum(jnp.sum(mixed * mixed, axis=1), "cb")
+    out_sq = _direct_rails(jnp.sum(mixed * mixed, axis=1))
     inv_out = lax.rsqrt(out_sq / D + eps)[:, None]
     return (mixed * inv_out * out_gain.astype(jnp.float32)).astype(jnp.bfloat16)
 

time: 222 us -> 222 us (level)
    psum x1 -> x0, blocking collectives: 5.67 us -> none  [body(): out_sq = lax.psum(jnp.sum(mixed * mixed, axis=1), 'cb')]
    unnamed x0 -> x1, blocking collectives: none -> 5.63 us
where the time goes in v1:
time: 222 us
  waiting for transfers between devices  169 us (76%)
  matrix products  15 us (7%)
  between operations  14.1 us (6%)
  blocking collectives  14 us (6%)
  other arithmetic  8.15 us (4%)
    psum x1, waiting for transfers between devices, body(): total_sq, gate_sum, up_sum = lax.psum((local_sq, gate_part, up_part), 'cb')  104 us
    reduce_scatter x1, waiting for transfers between devices, body(): down = lax.psum_scatter(partial_down, 'ra', scatter_dimension=0, tiled=True)  64.7 us
    psum x1, blocking collectives, body(): total_sq, gate_sum, up_sum = lax.psum((local_sq, gate_part, up_part), 'cb')  8.37 us
    dot_general x1, matrix products, body(): partial_down = jnp.dot(hidden, w_down, preferred_element_type=jnp.float32)  6.83 us
    unnamed x1, blocking collectives  5.63 us
    dot_general x1, matrix products, body(): up_part = jnp.dot(scaled, w_up, preferred_element_type=jnp.float32)  4.74 us
  transfers between devices with their start and end apart: 2, of which 2 were waited for; matrix products, arithmetic and copies ran while one was open for 2% of the time, Pallas kernels for 0%

profile of v1, /device:TPU:0, one launch (start us, length us, event | category | flops | bytes accessed | tf_op | source)
XLA Modules:
  0.0 222.0 jit_solution(258619855604880505)
XLA Ops:
  6.5 0.0 copy-start
  6.5 0.0 all-reduce.4.cloned.1.call-start
  6.5 0.8 convert_element_type.19
  7.4 1.0 copy-done
  8.4 0.0 copy-start.1
  8.4 0.0 copy-start.3
  8.4 4.7 %fusion.1 = f32[512,1408]{1,0:T(8,128)} fusion(bf16[1024,1408]{1,0:T(8,128)(2,1)S(1)} %copy-done, f32[1024]{0:T(1024)S(1)} %convert_element_type.19, bf16[512,1024]{1,0:T(8,128)(2,1)} %param.6), kind=kOutput, calls=%fused_computation.4 | convolution fusion | flops 1477967872 | bytes 6819840 | tf_op jit(solution)/shard_map/dot_general | solution.py:20
  13.1 0.0 copy-done.1
  13.1 0.0 copy-done.3
  13.1 3.5 %fusion.2 = f32[512,1408]{1,0:T(8,128)} fusion(bf16[1024,1408]{1,0:T(8,128)(2,1)S(1)} %copy-done.3, f32[1024]{0:T(1024)S(1)} %convert_element_type.19, bf16[512,1024]{1,0:T(8,128)(2,1)S(1)} %copy-done.1), kind=kOutput, calls=%fused_computation.5 | convolution fusion | flops 1477967872 | bytes 6819840 | tf_op jit(solution)/shard_map/dot_general | solution.py:19
  16.6 0.0 all-reduce.4.cloned.1.call-update
  16.6 0.0 reduce-scatter.2.cloned.1.call-start
  16.6 1.5 multiply_reduce_fusion
  18.1 8.4 %psum.22 = f32[512]{0:T(512)S(1)} all-reduce(f32[512]{0:T(512)S(1)} %multiply_reduce_fusion), channel_id=1, replica_groups=mesh['ra'=8,'cb'=4] {'cb'}, use_global_device_ids=true, to_apply=%region_2.0 | all-reduce | flops 512 | bytes 4096 | tf_op jit(solution)/shard_map/psum | solution.py:21
  26.5 104.0 %all-reduce.4.cloned.1.call-done = (f32[512,1408]{1,0:T(8,128)}, f32[512,1408]{1,0:T(8,128)}) async-done(((f32[512,1408]{1,0:T(8,128)}, f32[512,1408]{1,0:T(8,128)}), (f32[512,1408]{1,0:T(8,128)}, f32[512,1408]{1,0:T(8,128)})) %all-reduce.4.cloned.1.call-update) | async-done | bytes 5767184 | tf_op jit(solution)/shard_map/psum | solution.py:21
  130.5 6.8 %fusion = f32[512,1024]{1,0:T(8,128)} fusion(bf16[1408,1024]{1,0:T(8,128)(2,1)} %param.10, f32[512,1408]{1,0:T(8,128)} %get-tuple-element.5, f32[512,1408]{1,0:T(8,128)} %get-tuple-element.6, f32[512]{0:T(512)S(1)} %add_rsqrt_fusion), kind=kOutput, calls=%fused_computation.3 | convolution fusion | flops 1482162176 | bytes 10749952 | tf_op jit(solution)/shard_map/dot_general | solution.py:24
  137.4 0.0 copy-start.2
  137.4 0.0 copy-start.4
  137.4 0.0 reduce-scatter.2.cloned.1.call-update
  137.4 2.8 %convert_element_type.18 = f32[512,1024]{1,0:T(8,128)} convert(bf16[512,1024]{1,0:T(8,128)(2,1)} %param.6) | non-fusion elementwise | flops 524288 | bytes 3145728 | tf_op jit(solution)/shard_map/convert_element_type | solution.py:16
  140.2 0.0 copy-done.2
  140.2 0.0 copy-done.4
  140.2 0.6 dynamic-slice
  141.5 64.7 %reduce-scatter.2.cloned.1.call-done = f32[64,1024]{1,0:T(8,128)} async-done(((f32[512,1024]{1,0:T(8,128)}), f32[64,1024]{1,0:T(8,128)}) %reduce-scatter.2.cloned.1.call-update) | async-done | bytes 262160 | tf_op jit(solution)/shard_map/reduce_scatter | solution.py:27
  206.2 1.2 multiply_reduce_fusion.1
  207.4 0.2 dynamic-update-slice
  207.6 5.6 %all-reduce = f32[256]{0:T(256)S(1)} all-reduce(f32[256]{0:T(256)S(1)} %dynamic-update-slice), channel_id=2, replica_groups=mesh['ra'=8,'cb'=4] {'cb'}, use_global_device_ids=true, to_apply=%add | all-reduce | flops 256 | bytes 2048
  213.2 0.1 reshape.8
  213.4 1.8 multiply_convert_fusion.5
  (5 shorter events, 0.0 us)
Async XLA Ops:
  6.5 1.8 copy-start
  6.5 124.0 %all-reduce.4.cloned.1.call-start = ((), (), s32[]{:S(2)}) async-start(), calls=%async_computation.2 | async-start | bytes 11534336 | tf_op jit(solution)/shard_map/psum | solution.py:21
  8.4 4.7 %copy-start.1 = (bf16[512,1024]{1,0:T(8,128)(2,1)S(1)}, bf16[512,1024]{1,0:T(8,128)(2,1)}, u32[]{:S(2)}) copy-start(bf16[512,1024]{1,0:T(8,128)(2,1)} %param.6) | copy-start | bytes 3145732
  8.4 4.7 %copy-start.3 = (bf16[1024,1408]{1,0:T(8,128)(2,1)S(1)}, bf16[1024,1408]{1,0:T(8,128)(2,1)}, u32[]{:S(2)}) copy-start(bf16[1024,1408]{1,0:T(8,128)(2,1)} %param.8) | copy-start | bytes 8650756
  16.6 189.6 %reduce-scatter.2.cloned.1.call-start = ((), (), s32[]{:S(2)}) async-start(), calls=%async_computation.1 | async-start | bytes 2359296 | tf_op jit(solution)/shard_map/reduce_scatter | solution.py:27
  137.4 2.9 %copy-start.2 = (bf16[1024]{0:T(1024)(128)(2,1)S(1)}, bf16[1024]{0:T(1024)(128)(2,1)}, u32[]{:S(2)}) copy-start(bf16[1024]{0:T(1024)(128)(2,1)} %param.11) | copy-start | bytes 6148
  137.4 2.9 %copy-start.4 = (u32[32]{0:T(128)S(1)}, u32[32]{0:T(128)}, u32[]{:S(2)}) copy-start(u32[32]{0:T(128)} %constant.29) | copy-start | bytes 388
Sparse Core Ops, SparseCore 0:
  16.7 113.7 all-reduce.3
  137.5 68.6 reduce-scatter.1
